TPU v7x, 32 devices: a whole 2x2x4 slice. The times are simulated.
32 devices in a mesh: rep: 4 (over z), fs: 4 (over y, x), tp: 2 (over core).
Axes of the slice: x: 2, y: 2, z: 4, core: 2. Of those that a mesh axis runs over, the one named last changes fastest.
Arguments:
- inputs: bfloat16 [512, 2048], P(('rep', 'fs', 'tp')), may hold values from -6 to 6
- cotangent: bfloat16 [512, 2048], P(('rep', 'fs', 'tp')), may hold values from -6 to 6
- norm_gain: float32 [2048], replicated, may hold values from 0.1 to 1.9
- gate_weight: bfloat16 [2048, 2816], P(None, ('fs', 'tp')), may hold values from -0.125 to 0.125
- up_weight: bfloat16 [2048, 2816], P(None, ('fs', 'tp')), may hold values from -0.125 to 0.125
- down_weight: bfloat16 [2816, 2048], P(('fs', 'tp')), may hold values from -0.109375 to 0.109375
Outputs:
- input_grad: bfloat16 [512, 2048], P(('rep', 'fs', 'tp'))
- gain_grad: float32 [2048], replicated
- down_grad: float32 [2816, 2048], P(('fs', 'tp'), 'rep')
All inputs are finite; a program needn't handle non-finite values.
Results may differ from a plain program's by a relative error of at most 0.0066.
Values may be sent and summed in bfloat16 or wider, within the bound.
A program may use at most 64 MiB of HBM per device.

v0:
```python
import jax
import jax.numpy as jnp
from jax import lax
from jax.sharding import PartitionSpec as P

EPS = 1e-06


def across_tokens(left, right):
    return lax.dot_general(
        left, right, (((0,), (0,)), ((), ())), preferred_element_type=jnp.float32
    )


def across_columns(left, right):
    return lax.dot_general(
        left, right, (((1,), (1,)), ((), ())), preferred_element_type=jnp.float32
    )


def per_device(inputs, cotangent, norm_gain, gate_weight, up_weight, down_weight):
    whole_x, whole_dy = (
        lax.all_gather(inputs, ("fs", "tp"), axis=0, tiled=True),
        lax.all_gather(cotangent, ("fs", "tp"), axis=0, tiled=True),
    )
    xf = whole_x.astype(jnp.float32)
    inv = lax.rsqrt(jnp.mean(xf * xf, axis=-1, keepdims=True) + EPS)
    normed = xf * inv
    hidden_in = (normed * norm_gain).astype(jnp.bfloat16)
    gate = jnp.dot(hidden_in, gate_weight, preferred_element_type=jnp.float32)
    up = jnp.dot(hidden_in, up_weight, preferred_element_type=jnp.float32)
    sig = jax.nn.sigmoid(gate)
    act = gate * sig
    hidden = (act * up).astype(jnp.bfloat16)
    d_hidden = 0.5 * across_columns(whole_dy, down_weight)
    d_gate = (d_hidden * up * sig * (1.0 + gate * (1.0 - sig))).astype(jnp.bfloat16)
    d_up = (d_hidden * act).astype(jnp.bfloat16)
    own_rows = inputs.shape[0]
    d_in = lax.psum_scatter(
        across_columns(d_gate, gate_weight) + across_columns(d_up, up_weight),
        ("fs", "tp"),
        scatter_dimension=0,
        tiled=True,
    )
    offset = lax.axis_index(("fs", "tp")) * own_rows
    own_normed = lax.dynamic_slice_in_dim(normed, offset, own_rows, 0)
    own_inv = lax.dynamic_slice_in_dim(inv, offset, own_rows, 0)
    gain_grad = lax.psum(jnp.sum(d_in * own_normed, axis=0), ("rep", "fs", "tp"))
    scaled = d_in * norm_gain
    input_grad = (
        own_inv * (scaled - own_normed * jnp.mean(scaled * own_normed, axis=-1, keepdims=True))
    ).astype(jnp.bfloat16)
    input_grad, gain_grad = (input_grad, gain_grad)
    part_down = 0.5 * across_tokens(whole_dy, hidden)
    got_down = lax.all_to_all(
        part_down[None].astype(jnp.bfloat16), "rep", split_axis=1, concat_axis=0, tiled=True
    ).astype(jnp.float32)
    down_grad = jnp.sum(got_down, axis=0).T
    return (input_grad, gain_grad, down_grad)


def solution(mesh):
    return jax.shard_map(
        per_device,
        mesh=mesh,
        in_specs=(
            P(("rep", "fs", "tp"), None),
            P(("rep", "fs", "tp"), None),
            P(),
            P(None, ("fs", "tp")),
            P(None, ("fs", "tp")),
            P(("fs", "tp"), None),
        ),
        out_specs=(P(("rep", "fs", "tp"), None), P(), P(("fs", "tp"), "rep")),
        check_vma=False,
    )
```

profile of v0, /device:TPU:0, one launch (start us, length us, event | category | flops | bytes accessed | tf_op | source)
XLA Modules:
  0.0 166.7 jit_solution(2304956729085242355)
XLA Ops:
  7.2 0.0 copy-start
  7.2 0.0 reduce-scatter.2.cloned.1.call-start
  7.2 11.8 %all_gather.6 = bf16[128,2048]{1,0:T(8,128)(2,1)S(1)} all-gather(bf16[16,2048]{1,0:T(8,128)(2,1)} %param.6), channel_id=1, replica_groups=mesh['rep'=4,'fs'=4,'tp'=2] {'fs','tp'}, dimensions={0}, use_global_device_ids=true | all-gather | bytes 589824 | tf_op jit(solution)/shard_map/all_gather | solution.py:23
  19.0 0.0 copy-start.4
  19.0 0.0 copy-start.7
  19.0 0.2 fusion.2
  19.2 0.0 copy-done
  19.2 1.4 fusion.3
  20.6 0.0 copy-done.4
  20.6 0.0 copy-done.7
  20.6 0.0 copy-start.2
  20.6 0.0 copy-start.6
  20.7 0.0 copy-start.3
  20.7 0.6 fusion.4
  21.3 0.3 copy-done.6
  21.6 0.0 copy-start.5
  21.6 9.5 %all_gather.7 = bf16[128,2048]{1,0:T(8,128)(2,1)S(1)} all-gather(bf16[16,2048]{1,0:T(8,128)(2,1)S(1)} %copy-done.6), channel_id=1, replica_groups=mesh['rep'=4,'fs'=4,'tp'=2] {'fs','tp'}, dimensions={0}, use_global_device_ids=true | all-gather | bytes 589824 | tf_op jit(solution)/shard_map/all_gather | solution.py:24
  31.1 0.0 copy-start.1
  31.1 0.8 copy-done.1
  31.9 0.0 copy-done.3
  31.9 0.5 convolution_multiply_fusion.1
  32.4 0.5 fusion.6
  32.9 0.0 copy-done.2
  33.0 0.0 copy-done.5
  33.0 1.5 convolution_add_fusion
  34.5 0.0 reduce-scatter.2.cloned.1.call-update
  34.5 1.8 %fusion.1 = bf16[1,2048,352]{1,2,0:T(8,128)(2,1)S(1)} fusion(bf16[128,2048]{1,0:T(8,128)(2,1)} %copy-done.1, f32[128,352]{0,1:T(8,128)} %copy-done.5, f32[128,352]{0,1:T(8,128)} %copy-done.2), kind=kOutput, calls=%fused_computation.2 | convolution fusion | flops 186261504 | bytes 2326528 | tf_op jit(solution)/shard_map/dot_general | solution.py:10
  36.3 5.7 %copy.12 = bf16[1,2048,352]{2,0,1:T(2,128)(2,1)} copy(bf16[1,2048,352]{1,2,0:T(8,128)(2,1)S(1)} %fusion.1) | data formatting | bytes 2883584 | tf_op jit(solution)/shard_map/convert_element_type | solution.py:56
  42.0 0.5 broadcast.53
  42.5 34.4 %reduce = bf16[2048,352]{1,0:T(8,128)(2,1)S(1)} reduce(bf16[2048,1,352]{2,1,0:T(2,128)(2,1)} %bitcast.16, bf16[]{:T(256)} %broadcast.53), dimensions={1}, to_apply=%bitcast.7.reduce_sub_computation | reduce | bytes 2883586
  76.9 3.6 %reshape.41 = bf16[4,2,90112]{2,1,0:T(2,128)(2,1)} reshape(bf16[2048,352]{1,0:T(8,128)(2,1)S(1)} %reduce) | data formatting | bytes 2883584
  80.5 4.9 %all-to-all-start = ((bf16[4,2,90112]{2,1,0:T(2,128)(2,1)}), bf16[4,2,90112]{2,1,0:T(2,128)(2,1)S(1)}, u32[]{:S(2)}, u32[]{:S(2)}) async-start(bf16[4,2,90112]{2,1,0:T(2,128)(2,1)} %reshape.41), calls=%async_computation.1 | async-start | bytes 2883584 | tf_op jit(solution)/shard_map/all_to_all | solution.py:55
  85.3 0.1 dynamic-slice.3
  85.4 1.1 convert_multiply_fusion
  86.5 0.0 reduce-scatter.2.cloned.1.call-done
  86.5 1.1 multiply_reduce_fusion
  87.6 51.7 %psum.7 = f32[2048]{0:T(1024)} all-reduce(f32[2048]{0:T(1024)S(1)} %get-tuple-element.3), channel_id=1, replica_groups=mesh['rep'=4,'fs'=4,'tp'=2] {'rep','fs','tp'}, use_global_device_ids=true, to_apply=%region_4.0 | all-reduce | flops 2048 | bytes 16384 | tf_op jit(solution)/shard_map/psum | solution.py:48
  139.4 1.7 %multiply_convert_fusion.6 = bf16[16,2048]{1,0:T(8,128)(2,1)} fusion(f32[16,2048]{1,0:T(8,128)} %reduce-scatter.2.cloned.1.call-done, f32[128,2048]{1,0:T(8,128)} %convert_multiply_fusion, s32[]{:T(128)S(6)} %select_n.4, f32[16]{0:T(128)S(1)} %broadcast_multiply_fusion, f32[2048]{0:T(1024)S(1)} %copy-done.7, f32[16]{0:T(128)S(1)} %dynamic-slice.3), kind=kLoop, calls=%fused_computation.17 | loop fusion | flops 163840 | bytes 336004 | tf_op jit(solution)/shard_map/convert_element_type | solution.py:52
  141.0 0.0 all-to-all-done
  141.1 4.0 %reshape.42 = bf16[2048,1,352]{2,1,0:T(2,128)(2,1)} reshape(bf16[4,2,90112]{2,1,0:T(2,128)(2,1)S(1)} %all-to-all-done) | data formatting | bytes 2883584
  145.0 7.0 %copy.13 = bf16[1,2048,352]{1,2,0:T(8,128)(2,1)S(1)} copy(bf16[1,2048,352]{2,0,1:T(2,128)(2,1)} %bitcast.17) | data formatting | bytes 2883584 | tf_op jit(solution)/shard_map/all_to_all | solution.py:55
  152.0 3.4 %reshape.40 = f32[4,512,352]{1,0,2:T(4,128)} reshape(bf16[1,2048,352]{1,2,0:T(8,128)(2,1)S(1)} %copy.13) | data formatting | bytes 4325376 | tf_op jit(solution)/shard_map/convert_element_type | solution.py:57
  155.5 4.4 %reduce_sum.39 = f32[512,352]{0,1:T(8,128)} reduce(f32[4,512,352]{1,0,2:T(4,128)} %reshape.40, f32[]{:T(128)} %constant.11.clone.1), dimensions={0}, to_apply=%region_5.0 | reduce | flops 540672 | bytes 3604484 | tf_op jit(solution)/shard_map/reduce_sum | solution.py:58
  (2 shorter events, 0.0 us)
Async XLA Ops:
  7.2 12.0 %copy-start = (bf16[2048,352]{0,1:T(8,128)(2,1)S(1)}, bf16[2048,352]{0,1:T(8,128)(2,1)}, u32[]{:S(2)}) copy-start(bf16[2048,352]{0,1:T(8,128)(2,1)} %param.9) | copy-start | bytes 4325380
  7.2 79.3 %reduce-scatter.2.cloned.1.call-start = ((), (), s32[]{:S(2)}) async-start(), calls=%async_computation.2 | async-start | bytes 1179648 | tf_op jit(solution)/shard_map/reduce_scatter | solution.py:39
  19.0 1.6 copy-start.4
  19.0 1.6 copy-start.7
  20.6 12.3 %copy-start.2 = (f32[128,352]{0,1:T(8,128)}, f32[128,352]{0,1:T(8,128)S(1)}, u32[]{:S(2)}) copy-start(f32[128,352]{0,1:T(8,128)S(1)} %fusion.3) | copy-start | bytes 540676
  20.6 0.9 copy-start.6
  20.7 11.2 %copy-start.3 = (bf16[352,2048]{1,0:T(8,128)(2,1)S(1)}, bf16[352,2048]{1,0:T(8,128)(2,1)}, u32[]{:S(2)}) copy-start(bf16[352,2048]{1,0:T(8,128)(2,1)} %param.11) | copy-start | bytes 4325380
  21.6 11.4 %copy-start.5 = (f32[128,352]{0,1:T(8,128)}, f32[128,352]{0,1:T(8,128)S(1)}, u32[]{:S(2)}) copy-start(f32[128,352]{0,1:T(8,128)S(1)} %fusion.4) | copy-start | bytes 540676
  31.1 0.8 copy-start.1
  80.5 60.6 %all-to-all-start = ((bf16[4,2,90112]{2,1,0:T(2,128)(2,1)}), bf16[4,2,90112]{2,1,0:T(2,128)(2,1)S(1)}, u32[]{:S(2)}, u32[]{:S(2)}) async-start(bf16[4,2,90112]{2,1,0:T(2,128)(2,1)} %reshape.41), calls=%async_computation.1 | async-start | bytes 2883584 | tf_op jit(solution)/shard_map/all_to_all | solution.py:55
Sparse Core Ops, SparseCore 0:
  34.6 36.2 reduce-scatter.1
where the time goes:
time: 167 us
  blocking collectives  73 us (44%)
  other arithmetic  42.9 us (26%)
  local copies, waits for them, and re-layouts  25.4 us (15%)
  between operations  14.2 us (9%)
  matrix products  6.35 us (4%)
  starting transfers between devices  4.91 us (3%)
    psum x1, blocking collectives, per_device(): lax.psum(jnp.sum(d_in * own_normed, axis=0), ('rep', 'fs', 'tp'))  51.7 us
    unnamed x1, other arithmetic  34.4 us
    all_gather x1, blocking collectives, per_device(): lax.all_gather(inputs, ('fs', 'tp'), axis=0, tiled=True)  11.8 us
    all_gather x1, blocking collectives, per_device(): lax.all_gather(cotangent, ('fs', 'tp'), axis=0, tiled=True)  9.52 us
    unnamed x19, local copies, waits for them, and re-layouts  9.19 us
    all_to_all x1, local copies, waits for them, and re-layouts, per_device(): lax.all_to_all(part_down[None].astype(jnp.bfloat16), 'rep', split_axis=1,...  7.01 us
    convert_element_type x1, local copies, waits for them, and re-layouts, per_device(): part_down[None].astype(jnp.bfloat16)  5.72 us
    all_to_all x1, starting transfers between devices, per_device(): lax.all_to_all(part_down[None].astype(jnp.bfloat16), 'rep', split_axis=1,...  4.87 us
  transfers between devices with their start and end apart: 2, of which 0 were waited for; matrix products, arithmetic and copies ran while one was open for 30% of the time, Pallas kernels for 0%

commit v1 on v0

--- a/solution.py
+++ b/solution.py
@@ -45,7 +45,9 @@
     offset = lax.axis_index(("fs", "tp")) * own_rows
     own_normed = lax.dynamic_slice_in_dim(normed, offset, own_rows, 0)
     own_inv = lax.dynamic_slice_in_dim(inv, offset, own_rows, 0)
-    gain_grad = lax.psum(jnp.sum(d_in * own_normed, axis=0), ("rep", "fs", "tp"))
+    gain_grad = jnp.sum(
+        lax.all_gather(jnp.sum(d_in * own_normed, axis=0), ("rep", "fs", "tp")), axis=0
+    )
     scaled = d_in * norm_gain
     input_grad = (
         own_inv * (scaled - own_normed * jnp.mean(scaled * own_normed, axis=-1, keepdims=True))

time: 167 us -> 173 us (1.036)
  blocking collectives: 73 us -> 78.4 us
    all_gather x0 -> x1, blocking collectives: none -> 57.1 us  [per_device(): lax.all_gather(jnp.sum(d_in * own_normed, axis=0), ('rep', 'fs', 'tp'))]
    psum x1 -> x0, blocking collectives: 51.7 us -> none  [per_device(): lax.psum(jnp.sum(d_in * own_normed, axis=0), ('rep', 'fs', 'tp'))]
  transfers between devices with their start and end apart: 2 -> 2, of which waited for: 0 -> 0; matrix products, arithmetic and copies ran while one was open for 30% -> 29% of each run, Pallas kernels for 0% -> 0%
where the time goes in v1:
time: 173 us
  blocking collectives  78.4 us (45%)
  other arithmetic  43.5 us (25%)
  local copies, waits for them, and re-layouts  25.5 us (15%)
  between operations  14.2 us (8%)
  matrix products  6.35 us (4%)
  starting transfers between devices  4.91 us (3%)
    all_gather x1, blocking collectives, per_device(): lax.all_gather(jnp.sum(d_in * own_normed, axis=0), ('rep', 'fs', 'tp'))  57.1 us
    unnamed x1, other arithmetic  34.4 us
    all_gather x1, blocking collectives, per_device(): lax.all_gather(inputs, ('fs', 'tp'), axis=0, tiled=True)  11.8 us
    all_gather x1, blocking collectives, per_device(): lax.all_gather(cotangent, ('fs', 'tp'), axis=0, tiled=True)  9.52 us
    unnamed x19, local copies, waits for them, and re-layouts  9.19 us
    all_to_all x1, local copies, waits for them, and re-layouts, per_device(): lax.all_to_all(part_down[None].astype(jnp.bfloat16), 'rep', split_axis=1,...  7.01 us
    convert_element_type x1, local copies, waits for them, and re-layouts, per_device(): part_down[None].astype(jnp.bfloat16)  5.72 us
    all_to_all x1, starting transfers between devices, per_device(): lax.all_to_all(part_down[None].astype(jnp.bfloat16), 'rep', split_axis=1,...  4.87 us
  transfers between devices with their start and end apart: 2, of which 0 were waited for; matrix products, arithmetic and copies ran while one was open for 29% of the time, Pallas kernels for 0%

profile of v1, /device:TPU:0, one launch (start us, length us, event | category | flops | bytes accessed | tf_op | source)
XLA Modules:
  0.0 172.8 jit_solution(10523270191200942209)
XLA Ops:
  7.2 0.0 copy-start
  7.2 0.0 reduce-scatter.2.cloned.1.call-start
  7.2 11.8 %all_gather.12 = bf16[128,2048]{1,0:T(8,128)(2,1)S(1)} all-gather(bf16[16,2048]{1,0:T(8,128)(2,1)} %param.6), channel_id=1, replica_groups=mesh['rep'=4,'fs'=4,'tp'=2] {'fs','tp'}, dimensions={0}, use_global_device_ids=true | all-gather | bytes 589824 | tf_op jit(solution)/shard_map/all_gather | solution.py:23
  19.0 0.0 copy-start.4
  19.0 0.0 copy-start.7
  19.0 0.2 fusion.2
  19.2 0.0 copy-done
  19.2 1.4 fusion.3
  20.6 0.0 copy-done.4
  20.6 0.0 copy-done.7
  20.6 0.0 copy-start.2
  20.6 0.0 copy-start.6
  20.7 0.0 copy-start.3
  20.7 0.6 fusion.4
  21.3 0.3 copy-done.6
  21.6 0.0 copy-start.5
  21.6 9.5 %all_gather.13 = bf16[128,2048]{1,0:T(8,128)(2,1)S(1)} all-gather(bf16[16,2048]{1,0:T(8,128)(2,1)S(1)} %copy-done.6), channel_id=1, replica_groups=mesh['rep'=4,'fs'=4,'tp'=2] {'fs','tp'}, dimensions={0}, use_global_device_ids=true | all-gather | bytes 589824 | tf_op jit(solution)/shard_map/all_gather | solution.py:24
  31.1 0.0 copy-start.1
  31.1 0.8 copy-done.1
  31.9 0.0 copy-done.3
  31.9 0.5 convolution_multiply_fusion.1
  32.4 0.5 fusion.6
  32.9 0.0 copy-done.2
  33.0 0.0 copy-done.5
  33.0 1.5 convolution_add_fusion
  34.5 0.0 reduce-scatter.2.cloned.1.call-update
  34.5 1.8 %fusion.1 = bf16[1,2048,352]{1,2,0:T(8,128)(2,1)S(1)} fusion(bf16[128,2048]{1,0:T(8,128)(2,1)} %copy-done.1, f32[128,352]{0,1:T(8,128)} %copy-done.5, f32[128,352]{0,1:T(8,128)} %copy-done.2), kind=kOutput, calls=%fused_computation.2 | convolution fusion | flops 186261504 | bytes 2326528 | tf_op jit(solution)/shard_map/dot_general | solution.py:10
  36.3 5.7 %copy.14 = bf16[1,2048,352]{2,0,1:T(2,128)(2,1)} copy(bf16[1,2048,352]{1,2,0:T(8,128)(2,1)S(1)} %fusion.1) | data formatting | bytes 2883584 | tf_op jit(solution)/shard_map/convert_element_type | solution.py:58
  42.0 0.5 broadcast.53
  42.5 34.4 %reduce = bf16[2048,352]{1,0:T(8,128)(2,1)S(1)} reduce(bf16[2048,1,352]{2,1,0:T(2,128)(2,1)} %bitcast.16, bf16[]{:T(256)} %broadcast.53), dimensions={1}, to_apply=%bitcast.7.reduce_sub_computation | reduce | bytes 2883586
  76.9 3.6 %reshape.42 = bf16[4,2,90112]{2,1,0:T(2,128)(2,1)} reshape(bf16[2048,352]{1,0:T(8,128)(2,1)S(1)} %reduce) | data formatting | bytes 2883584
  80.5 4.9 %all-to-all-start = ((bf16[4,2,90112]{2,1,0:T(2,128)(2,1)}), bf16[4,2,90112]{2,1,0:T(2,128)(2,1)S(1)}, u32[]{:S(2)}, u32[]{:S(2)}) async-start(bf16[4,2,90112]{2,1,0:T(2,128)(2,1)} %reshape.42), calls=%async_computation.1 | async-start | bytes 2883584 | tf_op jit(solution)/shard_map/all_to_all | solution.py:57
  85.3 0.1 dynamic-slice.3
  85.4 1.1 convert_multiply_fusion
  86.5 0.0 reduce-scatter.2.cloned.1.call-done
  86.5 1.1 multiply_reduce_fusion
  87.6 57.1 %all-gather = f32[65536]{0:T(1024)S(1)} all-gather(f32[2048]{0:T(1024)S(1)} %get-tuple-element.3), channel_id=2, replica_groups=mesh['rep'=4,'fs'=4,'tp'=2] {'rep','fs','tp'}, dimensions={0}, use_global_device_ids=true | all-gather | bytes 270336 | tf_op jit(solution)/shard_map/all_gather | solution.py:49
  144.8 0.6 reduce_sum.48
  145.4 1.7 multiply_convert_fusion.6
  147.1 0.0 all-to-all-done
  147.1 4.0 %reshape.43 = bf16[2048,1,352]{2,1,0:T(2,128)(2,1)} reshape(bf16[4,2,90112]{2,1,0:T(2,128)(2,1)S(1)} %all-to-all-done) | data formatting | bytes 2883584
  151.1 7.0 %copy.15 = bf16[1,2048,352]{1,2,0:T(8,128)(2,1)S(1)} copy(bf16[1,2048,352]{2,0,1:T(2,128)(2,1)} %bitcast.17) | data formatting | bytes 2883584 | tf_op jit(solution)/shard_map/all_to_all | solution.py:57
  158.1 3.4 %reshape.40 = f32[4,512,352]{1,0,2:T(4,128)} reshape(bf16[1,2048,352]{1,2,0:T(8,128)(2,1)S(1)} %copy.15) | data formatting | bytes 4325376 | tf_op jit(solution)/shard_map/convert_element_type | solution.py:59
  161.5 4.4 %reduce_sum.49 = f32[512,352]{0,1:T(8,128)} reduce(f32[4,512,352]{1,0,2:T(4,128)} %reshape.40, f32[]{:T(128)} %constant.11.clone.1), dimensions={0}, to_apply=%region_5.0 | reduce | flops 540672 | bytes 3604484 | tf_op jit(solution)/shard_map/reduce_sum | solution.py:60
  (3 shorter events, 0.1 us)
Async XLA Ops:
  7.2 12.0 %copy-start = (bf16[2048,352]{0,1:T(8,128)(2,1)S(1)}, bf16[2048,352]{0,1:T(8,128)(2,1)}, u32[]{:S(2)}) copy-start(bf16[2048,352]{0,1:T(8,128)(2,1)} %param.9) | copy-start | bytes 4325380
  7.2 79.3 %reduce-scatter.2.cloned.1.call-start = ((), (), s32[]{:S(2)}) async-start(), calls=%async_computation.2 | async-start | bytes 1179648 | tf_op jit(solution)/shard_map/reduce_scatter | solution.py:39
  19.0 1.6 copy-start.4
  19.0 1.6 copy-start.7
  20.6 12.3 %copy-start.2 = (f32[128,352]{0,1:T(8,128)}, f32[128,352]{0,1:T(8,128)S(1)}, u32[]{:S(2)}) copy-start(f32[128,352]{0,1:T(8,128)S(1)} %fusion.3) | copy-start | bytes 540676
  20.6 0.9 copy-start.6
  20.7 11.2 %copy-start.3 = (bf16[352,2048]{1,0:T(8,128)(2,1)S(1)}, bf16[352,2048]{1,0:T(8,128)(2,1)}, u32[]{:S(2)}) copy-start(bf16[352,2048]{1,0:T(8,128)(2,1)} %param.11) | copy-start | bytes 4325380
  21.6 11.4 %copy-start.5 = (f32[128,352]{0,1:T(8,128)}, f32[128,352]{0,1:T(8,128)S(1)}, u32[]{:S(2)}) copy-start(f32[128,352]{0,1:T(8,128)S(1)} %fusion.4) | copy-start | bytes 540676
  31.1 0.8 copy-start.1
  80.5 66.6 %all-to-all-start = ((bf16[4,2,90112]{2,1,0:T(2,128)(2,1)}), bf16[4,2,90112]{2,1,0:T(2,128)(2,1)S(1)}, u32[]{:S(2)}, u32[]{:S(2)}) async-start(bf16[4,2,90112]{2,1,0:T(2,128)(2,1)} %reshape.42), calls=%async_computation.1 | async-start | bytes 2883584 | tf_op jit(solution)/shard_map/all_to_all | solution.py:57
Sparse Core Ops, SparseCore 0:
  34.6 36.2 reduce-scatter.1
